TPU v7x, 32 devices: a whole 2x2x4 slice. The times are simulated.
32 devices in a mesh: grp: 2 (over y), sp: 4 (over z), dp: 4 (over x, core).
Axes of the slice: x: 2, y: 2, z: 4, core: 2. Of those that a mesh axis runs over, the one named last changes fastest.
Arguments:
- mixer_source_array: bfloat16 [8, 768, 2048], P(('grp', 'dp'), 'sp'), parts along dimension 0, may hold values from -6 to 6
- source_projection: bfloat16 [2048, 1024], P('dp'), may hold values from -0.125 to 0.125
- gating_projection: bfloat16 [2048, 1024], P('dp'), may hold values from -0.125 to 0.125
- entry_mapping_projection: bfloat16 [2048, 256], replicated, may hold values from -0.0390625 to 0.0390625
- readout_mapping_projection: bfloat16 [2048, 256], replicated, may hold values from -0.0390625 to 0.0390625
- increment_projection: bfloat16 [2048, 16], replicated, may hold values from -0.125 to 0.125
- source_conv_taps: float32 [4, 1024], replicated, may hold values from -3 to 3
- entry_mapping_taps: float32 [4, 256], replicated, may hold values from -3 to 3
- readout_mapping_taps: float32 [4, 256], replicated, may hold values from -3 to 3
- increment_offsets: float32 [16], replicated, may hold values from -1 to 1
- channel_damping_rate: float32 [16], replicated, may hold values from 0 to 1
- bypass_coefficients: float32 [16], replicated, may hold values from 0.5 to 1.5
- stride_multiplier: float32 [8, 768], P(('grp', 'dp')), parts along dimension 0, may hold values from 0.5 to 2
- added_log_damping: float32 [8, 768, 16], P(('grp', 'dp')), parts along dimension 0, may hold values from -2.1 to 0
- norm_scale_factor: float32 [1024], replicated, may hold values from 0.1 to 1.9
- final_projection: bfloat16 [1024, 2048], P(None, 'dp'), may hold values from -0.1875 to 0.1875
Outputs:
- output: bfloat16 [8, 768, 2048], P(('grp', 'dp'), 'sp'), parts along dimension 0
There are 2 independent parts, one for each index of `grp`. A program takes and returns all parts, laid end to end along the dimension named above; an argument that names none is the same for every part. Nothing has to cross between parts.
All inputs are finite; a program needn't handle non-finite values.
Results may differ from a plain program's by a relative error of at most 0.015.
Values may be sent and summed in bfloat16 or wider, within the bound.
No kernel may reach another device: no remote copies, remote signals or barrier semaphores. Data moves between devices by JAX's collectives and lax.ppermute only.
A program may use at most 64 MiB of HBM per device.

v0:
```python
import jax
import jax.numpy as jnp
from jax import lax
from jax.sharding import PartitionSpec as P

P_SIZE = 64
N = 128
G = 2
CONV_W = 4
BLK = 64


EPSILON = 1e-06
HIGH = lax.Precision.HIGHEST


def conv_silu(padded, taps):
    width = taps.shape[0]
    length = padded.shape[0] - width + 1
    total = taps[0][None, :] * padded[0:length]
    for shift_pos in range(1, width):
        total = total + taps[shift_pos][None, :] * padded[shift_pos : shift_pos + length]
    return jax.nn.silu(total).astype(jnp.bfloat16)


def block_parts(x_blocks, b_blocks, c_blocks, step_width_value, logarithm_retain):
    cumulative = jnp.cumsum(logarithm_retain, axis=1)
    scaled = (x_blocks.astype(jnp.float32) * step_width_value[..., None]).astype(jnp.bfloat16)
    intersection = jnp.einsum(
        "kign,kjgn->kgij", c_blocks, b_blocks, preferred_element_type=jnp.float32
    )
    by_row = jnp.transpose(cumulative, (0, 2, 3, 1))
    log_gap = by_row[..., :, None] - by_row[..., None, :]
    length = log_gap.shape[-1]
    lower = jnp.tril(jnp.ones((length, length), bool))
    mixing = (intersection[:, :, None] * jnp.exp(jnp.where(lower, log_gap, -jnp.inf))).astype(
        jnp.bfloat16
    )
    inner = jnp.einsum("kgrij,kjgrp->kigrp", mixing, scaled, preferred_element_type=jnp.float32)
    to_end = jnp.exp(cumulative[:, -1:] - cumulative)
    weighted = (b_blocks[:, :, :, None, :].astype(jnp.float32) * to_end[..., None]).astype(
        jnp.bfloat16
    )
    states = jnp.einsum("kjgrn,kjgrp->kgrnp", weighted, scaled, preferred_element_type=jnp.float32)
    return (inner, states, cumulative[:, -1], cumulative)


def block_carry(states, block_total):
    incl_sum = jnp.cumsum(block_total, axis=0)
    excl_sum = incl_sum - block_total
    count = block_total.shape[0]
    log_gap = excl_sum[:, None] - incl_sum[None, :]
    before = (jnp.arange(count)[None, :] < jnp.arange(count)[:, None])[:, :, None, None]
    factors = jnp.exp(jnp.where(before, log_gap, -jnp.inf))
    carried = jnp.einsum("kjgr,jgrnp->kgrnp", factors, states, precision=HIGH)
    final_factor = jnp.exp(incl_sum[-1][None] - incl_sum)
    final_state = jnp.einsum("jgr,jgrnp->grnp", final_factor, states, precision=HIGH)
    return (carried, final_state, excl_sum, incl_sum[-1])


def block_finish(inner, c_blocks, cumulative, carried, x_blocks, skip):
    reached = jnp.einsum("kign,kgrnp->kigrp", c_blocks.astype(jnp.float32), carried, precision=HIGH)
    return (
        inner
        + reached * jnp.exp(cumulative)[..., None]
        + skip[..., None] * x_blocks.astype(jnp.float32)
    )


def heads_mixer(
    proj_x,
    proj_b,
    proj_c,
    step_raw,
    source_conv_taps,
    entry_mapping_taps,
    readout_mapping_taps,
    increment_offsets,
    channel_damping_rate,
    bypass_coefficients,
    tempo_row_values,
    surge_row_values,
):
    tok_rows = proj_x.shape[0]
    head_count = step_raw.shape[1]
    per_group = head_count // G
    shard_head_count = head_count // lax.axis_size("sp")
    leading_head_index = lax.axis_index("sp") * shard_head_count
    b_heads = jnp.broadcast_to(
        proj_b.reshape(tok_rows, G, 1, N), (tok_rows, G, per_group, N)
    ).reshape(tok_rows, head_count, N)
    c_heads = jnp.broadcast_to(
        proj_c.reshape(tok_rows, G, 1, N), (tok_rows, G, per_group, N)
    ).reshape(tok_rows, head_count, N)
    pairs = jnp.stack([b_heads, c_heads], axis=2).reshape(tok_rows, head_count * 2 * N)
    x_arrived, pairs_arrived, step_arrived = (
        lax.all_to_all(proj_x, "sp", split_axis=1, concat_axis=0, tiled=True),
        lax.all_to_all(pairs, "sp", split_axis=1, concat_axis=0, tiled=True),
        lax.all_to_all(step_raw, "sp", split_axis=1, concat_axis=0, tiled=True),
    )
    length = x_arrived.shape[0]
    head_ids = leading_head_index + jnp.arange(shard_head_count)
    group_pick = ((head_ids // per_group)[:, None] == jnp.arange(G)[None, :]).astype(jnp.float32)
    taps_x = lax.dynamic_slice_in_dim(
        source_conv_taps, leading_head_index * P_SIZE, shard_head_count * P_SIZE, 1
    )
    taps_b = jnp.einsum(
        "hg,wgn->whn", group_pick, entry_mapping_taps.reshape(CONV_W, G, N), precision=HIGH
    ).reshape(CONV_W, shard_head_count * N)
    taps_c = jnp.einsum(
        "hg,wgn->whn", group_pick, readout_mapping_taps.reshape(CONV_W, G, N), precision=HIGH
    ).reshape(CONV_W, shard_head_count * N)
    pair_parts = pairs_arrived.reshape(length, shard_head_count, 2, N)
    xs = conv_silu(
        jnp.concatenate(
            [
                jnp.zeros((CONV_W - 1, shard_head_count * P_SIZE), jnp.float32),
                x_arrived.astype(jnp.float32),
            ],
            0,
        ),
        taps_x,
    )
    b_rows = pair_parts[:, :, 0, :].reshape(length, shard_head_count * N).astype(jnp.float32)
    c_rows = pair_parts[:, :, 1, :].reshape(length, shard_head_count * N).astype(jnp.float32)
    bm = conv_silu(
        jnp.concatenate([jnp.zeros((CONV_W - 1, shard_head_count * N), jnp.float32), b_rows], 0),
        taps_b,
    )
    cm = conv_silu(
        jnp.concatenate([jnp.zeros((CONV_W - 1, shard_head_count * N), jnp.float32), c_rows], 0),
        taps_c,
    )
    bias_heads = lax.dynamic_slice_in_dim(
        increment_offsets, leading_head_index, shard_head_count, 0
    )
    speed_per_head = lax.dynamic_slice_in_dim(
        channel_damping_rate, leading_head_index, shard_head_count, 0
    )
    skip_heads = lax.dynamic_slice_in_dim(
        bypass_coefficients, leading_head_index, shard_head_count, 0
    )
    surge_head_values = lax.dynamic_slice_in_dim(
        surge_row_values, leading_head_index, shard_head_count, 1
    )
    step_width_value = jax.nn.softplus(step_arrived.astype(jnp.float32) + bias_heads[None, :])
    logarithm_retain = (
        -speed_per_head[None, :] * step_width_value * tempo_row_values[:, None] + surge_head_values
    )
    blocks = length // BLK
    x_blocks = xs.reshape(blocks, BLK, shard_head_count, 1, P_SIZE)
    b_blocks = bm.reshape(blocks, BLK, shard_head_count, N)
    c_blocks = cm.reshape(blocks, BLK, shard_head_count, N)
    inner, states, block_total, cumulative = block_parts(
        x_blocks,
        b_blocks,
        c_blocks,
        step_width_value.reshape(blocks, BLK, shard_head_count, 1),
        logarithm_retain.reshape(blocks, BLK, shard_head_count, 1),
    )
    carried, final_state, excl_sum, whole_total = block_carry(states, block_total)
    mixed = block_finish(
        inner, c_blocks, cumulative, carried, x_blocks, skip_heads.reshape(shard_head_count, 1)
    )
    mixed = mixed.astype(jnp.bfloat16).reshape(length, shard_head_count * P_SIZE)
    return lax.all_to_all(mixed, "sp", split_axis=0, concat_axis=1, tiled=True)


def shards(
    mixer_source_array,
    source_projection,
    gating_projection,
    entry_mapping_projection,
    readout_mapping_projection,
    increment_projection,
    source_conv_taps,
    entry_mapping_taps,
    readout_mapping_taps,
    increment_offsets,
    channel_damping_rate,
    bypass_coefficients,
    stride_multiplier,
    added_log_damping,
    norm_scale_factor,
    final_projection,
):
    hidden_width = mixer_source_array[0]
    tok_rows = hidden_width.shape[0]
    width_x = source_projection.shape[1]
    acc_x = jnp.dot(
        hidden_width,
        lax.all_gather(source_projection, "dp", axis=0, tiled=True),
        preferred_element_type=jnp.float32,
    )
    acc_z = jnp.dot(
        hidden_width,
        lax.all_gather(gating_projection, "dp", axis=0, tiled=True),
        preferred_element_type=jnp.float32,
    )
    proj_x = acc_x.astype(jnp.bfloat16)
    gate_z = acc_z.astype(jnp.bfloat16)
    proj_b = jnp.dot(
        hidden_width, entry_mapping_projection, preferred_element_type=jnp.float32
    ).astype(jnp.bfloat16)
    proj_c = jnp.dot(
        hidden_width, readout_mapping_projection, preferred_element_type=jnp.float32
    ).astype(jnp.bfloat16)
    step_raw = jnp.dot(
        hidden_width, increment_projection, preferred_element_type=jnp.float32
    ).astype(jnp.bfloat16)
    mixed = heads_mixer(
        proj_x,
        proj_b,
        proj_c,
        step_raw,
        source_conv_taps,
        entry_mapping_taps,
        readout_mapping_taps,
        increment_offsets,
        channel_damping_rate,
        bypass_coefficients,
        stride_multiplier[0],
        added_log_damping[0],
    )
    gated = mixed.astype(jnp.float32) * jax.nn.silu(gate_z.astype(jnp.float32))
    grouped = gated.reshape(tok_rows, G, width_x // G)
    normed = grouped * lax.rsqrt(jnp.mean(grouped * grouped, axis=-1, keepdims=True) + EPSILON)
    normed = (normed.reshape(tok_rows, width_x) * norm_scale_factor[None, :]).astype(jnp.bfloat16)
    output = jnp.dot(
        normed,
        lax.all_gather(final_projection, "dp", axis=1, tiled=True),
        preferred_element_type=jnp.float32,
    ).astype(jnp.bfloat16)
    return output[None]


def solution(mesh):
    return jax.shard_map(
        shards,
        mesh=mesh,
        in_specs=(
            P(("grp", "dp"), "sp", None),
            P("dp", None),
            P("dp", None),
            P(),
            P(),
            P(),
            P(),
            P(),
            P(),
            P(),
            P(),
            P(),
            P(("grp", "dp"), None),
            P(("grp", "dp"), None, None),
            P(),
            P(None, "dp"),
        ),
        out_specs=P(("grp", "dp"), "sp", None),
        check_vma=False,
    )
```

profile of v0, /device:TPU:0, one launch (start us, length us, event | category | flops | bytes accessed | tf_op | source)
XLA Modules:
  0.0 153.6 jit_solution(1723847888486538169)
XLA Ops:
  6.5 0.7 all-gather.4.cloned.1.call-update
  7.3 0.7 all-gather.6.cloned.1.call-update
  8.3 0.6 all_to_all.44
  9.0 6.3 %all-to-all-start.1 = ((bf16[192,4,4]{0,2,1:T(4,128)(2,1)}), bf16[192,4,4]{0,2,1:T(4,128)(2,1)S(1)}, u32[]{:S(2)}, u32[]{:S(2)}) async-start(bf16[192,4,4]{0,2,1:T(4,128)(2,1)} %all_to_all.44), calls=%async_computation.1 | async-start | bytes 16384 | tf_op jit(solution)/shard_map/all_to_all | solution.py:99
  15.3 0.7 all-gather.8.cloned.1.call-update
  16.1 0.4 convolution_convert_fusion.4
  16.6 0.4 convolution_convert_fusion.3
  17.0 0.8 constant_dynamic-slice_fusion.1
  18.4 0.9 constant_dynamic-slice_fusion
  19.6 3.6 %copy.109 = bf16[192,16,2,128]{3,2,1,0:T(2,128)(2,1)} copy(bf16[192,16,2,128]{3,1,0,2:T(8,128)(2,1)S(1)} %pad_maximum_fusion) | data formatting | bytes 3145728 | tf_op jit(solution)/shard_map/stack | solution.py:95
  23.3 2.4 %all_to_all.46 = bf16[192,4,1024]{2,1,0:T(4,128)(2,1)S(1)} reshape(bf16[192,16,2,128]{3,2,1,0:T(2,128)(2,1)} %copy.109) | data formatting | bytes 3145728 | tf_op jit(solution)/shard_map/all_to_all | solution.py:98
  25.6 1.6 %copy.110 = bf16[192,4,1024]{2,0,1:T(8,128)(2,1)} copy(bf16[192,4,1024]{2,1,0:T(4,128)(2,1)S(1)} %all_to_all.46) | data formatting | bytes 3145728 | tf_op jit(solution)/shard_map/all_to_all | solution.py:98
  27.4 5.1 %all-to-all-start.2 = ((bf16[192,4,1024]{2,0,1:T(8,128)(2,1)}), bf16[192,4,1024]{2,0,1:T(8,128)(2,1)}, u32[]{:S(2)}, u32[]{:S(2)}) async-start(bf16[192,4,1024]{2,0,1:T(8,128)(2,1)} %copy.110), calls=%async_computation.2 | async-start | bytes 3145728 | tf_op jit(solution)/shard_map/all_to_all | solution.py:98
  32.9 2.2 %copy.114 = f32[12,64,4,1]{3,0,1,2:T(8,128)} copy(f32[12,64,4,1]{1,0,2,3:T(8,128)S(1)} %fusion.40) | data formatting | bytes 24576 | tf_op jit(solution)/shard_map/add | solution.py:148
  35.0 1.8 %fusion.57 = f32[12,64,4,1]{3,0,1,2:T(8,128)S(1)} fusion(f32[12,64,4,1]{3,0,1,2:T(8,128)} %copy.114), kind=kOutput, calls=%fused_computation.106 | output fusion | flops 193536 | bytes 24576 | tf_op jit(solution)/shard_map/jit(cumsum)/reduce_window_sum | solution.py:27
  36.9 0.9 copy.119
  38.5 0.9 copy.108
  39.5 0.9 copy.115
  40.4 28.5 %all-to-all-done.2 = bf16[192,4,1024]{2,0,1:T(8,128)(2,1)} async-done(((bf16[192,4,1024]{2,0,1:T(8,128)(2,1)}), bf16[192,4,1024]{2,0,1:T(8,128)(2,1)}, u32[]{:S(2)}, u32[]{:S(2)}) %all-to-all-start.2) | async-done | bytes 1572896 | tf_op jit(solution)/shard_map/all_to_all | solution.py:98
  69.0 2.8 %reshape.304 = bf16[768,4,2,128]{3,2,1,0:T(2,128)(2,1)S(1)} reshape(bf16[4,192,1024]{2,1,0:T(8,128)(2,1)} %bitcast.14) | data formatting | bytes 3145728 | tf_op jit(solution)/shard_map/reshape | solution.py:113
  71.8 9.9 %fusion.7 = (f32[768,4,128]{2,1,0:T(4,128)}, f32[768,4,128]{2,1,0:T(4,128)S(1)}) fusion(bf16[768,4,2,128]{3,2,1,0:T(2,128)(2,1)S(1)} %reshape.304), kind=kLoop, calls=%fused_computation.10 | loop fusion | flops 786432 | bytes 4718592 | tf_op jit(solution)/shard_map/convert_element_type | solution.py:125
  81.8 1.0 copy-done.3
  82.8 3.2 %convolution_convert_fusion.2 = bf16[192,1024]{1,0:T(8,128)(2,1)S(1)} fusion(bf16[2048,1024]{1,0:T(8,128)(2,1)} %all-gather.4.cloned.1.call-done, bf16[1,192,2048]{2,1,0:T(8,128)(2,1)S(1)} %copy-done.3), kind=kOutput, calls=%fused_computation.29 | convolution fusion | flops 805502976 | bytes 5373952 | tf_op jit(solution)/shard_map/dot_general | solution.py:190
  86.0 0.8 copy.161
  86.7 4.3 %all-to-all-start = ((bf16[192,4,256]{2,0,1:T(8,128)(2,1)}), bf16[192,4,256]{2,0,1:T(8,128)(2,1)}, u32[]{:S(2)}, u32[]{:S(2)}) async-start(bf16[192,4,256]{2,0,1:T(8,128)(2,1)} %bitcast.130), calls=%async_computation | async-start | bytes 786432 | tf_op jit(solution)/shard_map/all_to_all | solution.py:97
  91.1 1.0 multiply_convert_fusion.2
  92.1 1.1 reshape.307
  93.2 0.8 copy-done.4
  94.1 1.0 multiply_convert_fusion.3
  95.1 1.1 reshape.305
  96.2 6.0 %all-to-all-done = bf16[192,4,256]{2,0,1:T(8,128)(2,1)} async-done(((bf16[192,4,256]{2,0,1:T(8,128)(2,1)}), bf16[192,4,256]{2,0,1:T(8,128)(2,1)}, u32[]{:S(2)}, u32[]{:S(2)}) %all-to-all-start) | async-done | bytes 393248 | tf_op jit(solution)/shard_map/all_to_all | solution.py:97
  102.2 1.1 convert_element_type.183
  103.2 0.5 fusion.37
  103.7 1.9 %reshape.310 = f32[12,64,4,64]{3,2,1,0:T(4,128)} reshape(f32[768,256]{1,0:T(8,128)S(1)} %fusion.37) | data formatting | bytes 1572864 | tf_op jit(solution)/shard_map/convert_element_type | solution.py:28
  105.6 0.7 reshape.315
  106.3 2.2 %multiply_convert_fusion.4 = bf16[12,64,4,64]{3,2,1,0:T(4,128)(2,1)S(1)} fusion(f32[12,64,4,64]{3,2,1,0:T(4,128)} %reshape.310, f32[12,64,4]{2,1,0:T(8,128)} %copy.108), kind=kLoop, calls=%fused_computation.26 | loop fusion | flops 393216 | bytes 1191936 | tf_op jit(solution)/shard_map/convert_element_type | solution.py:28
  108.4 1.2 copy.116
  109.6 1.6 %copy.125 = f32[12,64,4,1,64]{1,4,2,0,3:T(8,128)} copy(f32[12,64,4,1,64]{4,2,1,0,3:T(4,128)S(1)} %reshape.315) | data formatting | bytes 1572864 | tf_op jit(solution)/shard_map/convert_element_type | solution.py:28
  111.2 1.7 %fusion.16 = f32[12,4,128,64]{2,3,1,0:T(8,128)S(1)} fusion(bf16[12,64,4,64]{1,3,2,0:T(8,128)(2,1)} %copy.116, f32[12,64,4]{1,2,0:T(4,128)S(1)} %get-tuple-element.10, bf16[12,64,4,128]{3,2,1,0:T(4,128)(2,1)S(1)} %copy-done.5), kind=kOutput, calls=%fused_computation.35 | convolution fusion | flops 51511296 | bytes 2764800 | tf_op jit(solution)/shard_map/kjgrn,kjgrp->kgrnp/dot_general | solution.py:44
  113.0 3.1 %fusion.3 = f32[12,4,128,64]{2,0,3,1:T(8,128)S(1)} fusion(f32[12,4,128,64]{2,3,1,0:T(8,128)S(1)} %fusion.16, f32[12,4]{0,1:T(4,128)S(1)} %bitcast.144, f32[12,4]{0,1:T(4,128)S(1)} %get-tuple-element.7, pred[12,12]{1,0:T(8,128)(4,1)S(1)} %iota_compare_fusion.1), kind=kOutput, calls=%fused_computation.4 | convolution fusion | flops 56624256 | bytes 3146256 | tf_op jit(solution)/shard_map/kjgr,jgrnp->kgrnp/dot_general | solution.py:55
  116.1 2.9 %fusion.11 = f32[12,4,64,64]{3,2,1,0:T(8,128)} fusion(f32[12,4,128,64]{2,0,3,1:T(8,128)S(1)} %fusion.3, bf16[12,64,4,128]{3,2,1,0:T(4,128)(2,1)S(1)} %copy-done.7), kind=kOutput, calls=%fused_computation.16 | convolution fusion | flops 301989888 | bytes 3145728 | tf_op jit(solution)/shard_map/kign,kgrnp->kigrp/dot_general | solution.py:62
  119.0 3.3 %fusion.10 = bf16[12,64,4,1,64]{1,4,2,0,3:T(8,128)(2,1)} fusion(f32[12,4,64,64]{3,2,1,0:T(8,128)} %fusion.11, f32[12,64,4,1,64]{1,4,2,0,3:T(8,128)} %copy.125, bf16[12,64,4,64]{1,3,2,0:T(8,128)(2,1)S(1)} %copy-done.6, f32[4]{0:T(128)S(1)} %dynamic_slice.22, f32[12,64,4]{1,2,0:T(4,128)S(1)} %get-tuple-element.9, f32[12,4,64]{2,1,0:T(4,128)S(1)} %bitcast.142, ...), kind=kOutput, calls=%fused_computation.15 | convolution fusion | flops 77266944 | bytes 3960848 | tf_op jit(solution)/shard_map/kgrij,kjgrp->kigrp/dot_general | solution.py:39
  122.3 1.5 copy.126
  123.8 0.5 all_to_all.49
  124.3 13.7 %all_to_all.55 = bf16[4,192,256]{2,1,0:T(8,128)(2,1)S(1)} all-to-all(bf16[4,192,256]{2,1,0:T(8,128)(2,1)S(1)} %all_to_all.49), channel_id=1, replica_groups=mesh['grp'=2,'sp'=4,'dp'=4] {'sp'}, dimensions={0} | all-to-all | bytes 786432 | tf_op jit(solution)/shard_map/all_to_all | solution.py:166
  138.1 3.3 %fusion.56 = (f32[192,1024]{1,0:T(8,128)S(1)}, f32[192,1024]{1,0:T(8,128)S(1)}) fusion(f32[192,1024]{1,0:T(8,128)S(1)} %bitcast.139, bf16[2048,1024]{1,0:T(8,128)(2,1)} %all-gather.6.cloned.1.call-done, bf16[1,192,2048]{2,1,0:T(8,128)(2,1)S(1)} %copy-done.3), kind=kOutput, calls=%fused_computation.105 | convolution fusion | flops 806879232 | bytes 7340032 | tf_op jit(solution)/shard_map/dot_general | solution.py:195
  141.4 0.7 mul.310
  142.9 4.1 %fusion = bf16[1,192,2048]{2,1,0:T(8,128)(2,1)} fusion(bf16[1024,2048]{1,0:T(8,128)(2,1)} %all-gather.8.cloned.1.call-done, f32[192,1024]{1,0:T(8,128)S(1)} %get-tuple-element.24, f32[192,1024]{1,0:T(8,128)S(1)} %bitcast.138, f32[1024]{0:T(1024)S(1)} %copy-done.12), kind=kOutput, calls=%fused_computation.1 | convolution fusion | flops 806289408 | bytes 6557696 | tf_op jit(solution)/shard_map/dot_general | solution.py:229
  (79 shorter events, 4.1 us)
Async XLA Ops:
  6.5 9.6 %copy-start = (bf16[2048,256]{1,0:T(8,128)(2,1)S(1)}, bf16[2048,256]{1,0:T(8,128)(2,1)}, u32[]{:S(2)}) copy-start(bf16[2048,256]{1,0:T(8,128)(2,1)} %param.19) | copy-start | bytes 3145732
  6.5 1.5 copy-start.2
  6.5 1.5 copy-start.9
  6.5 75.3 %all-gather.4.cloned.1.call-start = ((), (), s32[]{:S(2)}) async-start(), calls=%async_computation.4 | async-start | bytes 5242880 | tf_op jit(solution)/shard_map/all_gather | solution.py:192
  7.3 8.8 %copy-start.10 = (f32[4,256]{1,0:T(4,128)S(1)}, f32[4,256]{1,0:T(4,128)}, u32[]{:S(2)}) copy-start(f32[4,256]{1,0:T(4,128)} %param.23) | copy-start | bytes 12292
  7.3 130.9 %all-gather.6.cloned.1.call-start = ((), (), s32[]{:S(2)}) async-start(), calls=%async_computation.5 | async-start | bytes 5242880 | tf_op jit(solution)/shard_map/all_gather | solution.py:197
  9.0 18.4 %all-to-all-start.1 = ((bf16[192,4,4]{0,2,1:T(4,128)(2,1)}), bf16[192,4,4]{0,2,1:T(4,128)(2,1)S(1)}, u32[]{:S(2)}, u32[]{:S(2)}) async-start(bf16[192,4,4]{0,2,1:T(4,128)(2,1)} %all_to_all.44), calls=%async_computation.1 | async-start | bytes 16384 | tf_op jit(solution)/shard_map/all_to_all | solution.py:99
  15.3 1.2 copy-start.8
  15.3 127.5 %all-gather.8.cloned.1.call-start = ((), (), s32[]{:S(2)}) async-start(), calls=%async_computation.6 | async-start | bytes 5242880 | tf_op jit(solution)/shard_map/all_gather | solution.py:231
  18.2 1.1 copy-start.14
  18.2 1.2 copy-start.15
  18.2 1.3 copy-start.13
  25.6 1.6 %copy-start.11 = (f32[4,256]{1,0:T(4,128)S(1)}, f32[4,256]{1,0:T(4,128)}, u32[]{:S(2)}) copy-start(f32[4,256]{1,0:T(4,128)} %param.24) | copy-start | bytes 12292
  25.6 1.7 %copy-start.16 = (f32[16]{0:T(128)S(1)}, f32[16]{0:T(128)}, u32[]{:S(2)}) copy-start(f32[16]{0:T(128)} %param.27) | copy-start | bytes 196
  27.4 41.6 %all-to-all-start.2 = ((bf16[192,4,1024]{2,0,1:T(8,128)(2,1)}), bf16[192,4,1024]{2,0,1:T(8,128)(2,1)}, u32[]{:S(2)}, u32[]{:S(2)}) async-start(bf16[192,4,1024]{2,0,1:T(8,128)(2,1)} %copy.110), calls=%async_computation.2 | async-start | bytes 3145728 | tf_op jit(solution)/shard_map/all_to_all | solution.py:98
  81.7 1.1 copy-start.3
  86.7 15.4 %all-to-all-start = ((bf16[192,4,256]{2,0,1:T(8,128)(2,1)}), bf16[192,4,256]{2,0,1:T(8,128)(2,1)}, u32[]{:S(2)}, u32[]{:S(2)}) async-start(bf16[192,4,256]{2,0,1:T(8,128)(2,1)} %bitcast.130), calls=%async_computation | async-start | bytes 786432 | tf_op jit(solution)/shard_map/all_to_all | solution.py:97
  92.1 1.9 %copy-start.4 = (f32[768,4,128]{2,1,0:T(4,128)S(1)}, f32[768,4,128]{2,1,0:T(4,128)}, u32[]{:S(2)}) copy-start(f32[768,4,128]{2,1,0:T(4,128)} %get-tuple-element.5) | copy-start | bytes 4718596
  109.6 1.6 %copy-start.5 = (bf16[12,64,4,128]{3,2,1,0:T(4,128)(2,1)S(1)}, bf16[12,64,4,128]{3,2,1,0:T(4,128)(2,1)}, u32[]{:S(2)}) copy-start(bf16[12,64,4,128]{3,2,1,0:T(4,128)(2,1)} %reshape.307) | copy-start | bytes 2359300
  113.0 3.1 %copy-start.7 = (bf16[12,64,4,128]{3,2,1,0:T(4,128)(2,1)S(1)}, bf16[12,64,4,128]{3,2,1,0:T(4,128)(2,1)}, u32[]{:S(2)}) copy-start(bf16[12,64,4,128]{3,2,1,0:T(4,128)(2,1)} %reshape.305) | copy-start | bytes 2359300
  116.1 2.9 %copy-start.6 = (bf16[12,64,4,64]{1,3,2,0:T(8,128)(2,1)S(1)}, bf16[12,64,4,64]{1,3,2,0:T(8,128)(2,1)}, u32[]{:S(2)}) copy-start(bf16[12,64,4,64]{1,3,2,0:T(8,128)(2,1)} %copy.116) | copy-start | bytes 1179652
  142.1 0.8 copy-start.12
  142.9 4.2 %copy-start.1 = (bf16[2048,256]{1,0:T(8,128)(2,1)S(1)}, bf16[2048,256]{1,0:T(8,128)(2,1)}, u32[]{:S(2)}) copy-start(bf16[2048,256]{1,0:T(8,128)(2,1)} %param.19) | copy-start | bytes 3145732
Sparse Core Ops, SparseCore 0:
  8.9 37.1 all-gather.3
  47.7 34.4 all-gather.5
  83.7 34.4 all-gather.7
where the time goes:
time: 155 us; the launch traced here: 154 us
  waiting for transfers between devices  36.7 us (24%)
  local copies, waits for them, and re-layouts  32.3 us (21%)
  matrix products  23 us (15%)
  other arithmetic  18.4 us (12%)
  starting transfers between devices  15.8 us (10%)
  blocking collectives  13.7 us (9%)
  between operations  13.6 us (9%)
    all_to_all x1, waiting for transfers between devices, heads_mixer(): lax.all_to_all(pairs, 'sp', split_axis=1, concat_axis=0, tiled=True)  28.5 us
    all_to_all x1, blocking collectives, heads_mixer(): return lax.all_to_all(mixed, 'sp', split_axis=0, concat_axis=1, tiled=True)  13.7 us
    convert_element_type x1, other arithmetic, heads_mixer(): pair_parts[:, :, 1, :].reshape(length, shard_head_count * N)  9.87 us
    all_to_all x1, starting transfers between devices, heads_mixer(): lax.all_to_all(step_raw, 'sp', split_axis=1, concat_axis=0, tiled=True)  6.35 us
    all_to_all x1, waiting for transfers between devices, heads_mixer(): lax.all_to_all(proj_x, 'sp', split_axis=1, concat_axis=0, tiled=True)  6.02 us
    all_to_all x1, starting transfers between devices, heads_mixer(): lax.all_to_all(pairs, 'sp', split_axis=1, concat_axis=0, tiled=True)  5.09 us
    all_to_all x1, starting transfers between devices, heads_mixer(): lax.all_to_all(proj_x, 'sp', split_axis=1, concat_axis=0, tiled=True)  4.35 us
    dot_general x1, matrix products, shards(): jnp.dot(normed, lax.all_gather(final_projection, 'dp', axis=1, tiled=True...  4.15 us
  transfers between devices with their start and end apart: 6, of which 2 were waited for; matrix products, arithmetic and copies ran while one was open for 42% of the time, Pallas kernels for 0%

commit v1 on v0

v1 whole, which is shorter than its diff:
```python
import functools

import jax
import jax.numpy as jnp
from jax import lax
from jax.experimental import pallas as pl
from jax.experimental.pallas import tpu as pltpu
from jax.sharding import PartitionSpec as P


N = 128
G = 2
HALO = 16
EPSILON = 1e-06
HIGH = lax.Precision.HIGHEST
F32 = jnp.float32
BF16 = jnp.bfloat16
SDS = jax.ShapeDtypeStruct


def dot(a, b, precision=None):
    return jnp.dot(a, b, preferred_element_type=F32, precision=precision)


def dot_t(a, b):
    return lax.dot_general(a, b, (((1,), (1,)), ((), ())), preferred_element_type=F32)


def dot_tl(a, b, precision=None):
    return lax.dot_general(
        a, b, (((0,), (0,)), ((), ())), preferred_element_type=F32, precision=precision
    )


def silu(v):
    return v / (1.0 + jnp.exp(-v))


def conv_silu(ref, first, taps, rows):
    width = taps.shape[0]
    first = first + HALO - (width - 1)
    total = taps[0:1, :] * ref[pl.ds(first, rows), :]
    for k in range(1, width):
        total = total + taps[k : k + 1, :] * ref[pl.ds(first + k, rows), :]
    return silu(total).astype(BF16)


def aligned(index, size):
    return pl.ds(pl.multiple_of(index * size, size), size)


def my_group():
    return lax.rem(lax.axis_index("dp"), G)


def maps_kernel(
    x_ref,
    wb_ref,
    wc_ref,
    wdt_ref,
    taps_b_ref,
    taps_c_ref,
    offset_ref,
    rate_ref,
    stride0_ref,
    stride1_ref,
    added0_ref,
    added1_ref,
    bm_ref,
    cm_ref,
    mix_ref,
    step_ref,
    send_ref,
    reach_ref,
    total_ref,
    pad_ref,
):
    c = my_group()
    place = lax.axis_index("sp")
    spans = lax.axis_size("sp")
    full = x_ref.shape[0] // 2
    rows = full - HALO
    heads = wdt_ref.shape[0] // G
    width = step_ref.shape[1]
    mine = aligned(c, N)
    for w_ref, taps_ref, out_ref in ((wb_ref, taps_b_ref, bm_ref), (wc_ref, taps_c_ref, cm_ref)):
        pad_ref[...] = dot(x_ref[...], w_ref[:, mine]).astype(BF16).astype(F32)
        for q in range(2):
            out_ref[q * rows : (q + 1) * rows, :] = conv_silu(
                pad_ref, q * full, taps_ref[:, mine], rows
            )
    src = lax.broadcasted_iota(jnp.int32, (rows, rows), 0)
    dst = lax.broadcasted_iota(jnp.int32, (rows, rows), 1)
    upper = (src <= dst).astype(F32)
    eye = (
        lax.broadcasted_iota(jnp.int32, (heads, heads), 0)
        == lax.broadcasted_iota(jnp.int32, (heads, heads), 1)
    ).astype(F32)
    spread = (
        lax.broadcasted_iota(jnp.int32, (heads, width), 1) // (width // heads)
        == lax.broadcasted_iota(jnp.int32, (heads, width), 0)
    ).astype(F32)
    head = lax.broadcasted_iota(jnp.int32, (heads, 1), 0)
    offset = jnp.zeros((heads, 1), F32)
    rate = jnp.zeros((heads, 1), F32)
    for r in range(heads):
        offset = jnp.where(head == r, offset_ref[c * heads + r], offset)
        rate = jnp.where(head == r, rate_ref[c * heads + r], rate)
    wdt = wdt_ref[aligned(c, heads), :]

    def own_span(ref, sub):
        picked = ref[sub, 0:rows]
        for s in range(1, spans):
            picked = jnp.where(place == s, ref[sub, s * rows : (s + 1) * rows], picked)
        return picked

    for q, (stride_ref, added_ref) in enumerate(
        ((stride0_ref, added0_ref), (stride1_ref, added1_ref))
    ):
        out = slice(q * rows, (q + 1) * rows)
        x_rows = x_ref[q * full + HALO : (q + 1) * full, :]
        raw = dot_t(wdt, x_rows).astype(BF16).astype(F32)
        shifted = raw + offset
        step_t = jnp.maximum(shifted, 0.0) + jnp.log1p(jnp.exp(-jnp.abs(shifted)))
        stride = own_span(stride_ref, slice(0, 1))
        added = own_span(added_ref, aligned(c, heads))
        keep_t = -rate * step_t * stride + added
        cum_t = dot(keep_t, upper, HIGH)
        total_t = cum_t[:, rows - 1 : rows]
        cum = dot_tl(cum_t, eye, HIGH)
        step_ref[out, :] = dot_tl(step_t, spread, HIGH)
        send_ref[out, :] = dot_tl(step_t * jnp.exp(total_t - cum_t), spread, HIGH)
        reach_ref[out, :] = dot_tl(jnp.exp(cum_t), spread, HIGH)
        total_ref[q * 8 : (q + 1) * 8, :] = dot_tl(
            jnp.broadcast_to(total_t, (heads, 8)), spread, HIGH
        )
        gram = jnp.where(src >= dst, dot_t(cm_ref[out, :], bm_ref[out, :]), 0.0)
        for r in range(heads):
            gap = cum[:, r : r + 1] - cum_t[r : r + 1, :]
            mix_ref[q * heads + r] = (gram * jnp.exp(jnp.minimum(gap, 0.0))).astype(BF16)


def shard_of(shift, flip):
    size = lax.axis_size("dp")
    return lax.rem(lax.axis_index("dp") - shift + size, size) ^ flip


def half_of(part):
    g = lax.axis_index("grp")
    return g if part == 0 else 1 - g


def proj_pieces(x_ref, refs, kinds, rows_w):
    total = None
    c = my_group()
    for ref, (shift, flip, part) in zip(refs, kinds):
        depth, lanes = ref.shape
        index = shard_of(shift, flip) * (rows_w // depth)
        if part is not None:
            index = index + half_of(part)
        w = ref[...] if (shift, flip) != (0, 0) else ref[:, aligned(c, lanes // G)]
        piece = dot(x_ref[:, aligned(index, depth)], w)
        total = piece if total is None else total + piece
    return total


def source_kernel(kinds, rows_w, *refs):
    x_ref, taps_ref, step_ref, send_ref, bm_ref = refs[:5]
    pieces = refs[5 : 5 + len(kinds)]
    xs_ref, scaled_ref, state_ref, state_bf_ref, pad_ref = refs[5 + len(kinds) :]
    full = x_ref.shape[0] // 2
    rows = full - HALO
    pad_ref[...] = proj_pieces(x_ref, pieces, kinds, rows_w).astype(BF16).astype(F32)
    taps = taps_ref[:, aligned(my_group(), pad_ref.shape[1])]
    for q in range(2):
        out = slice(q * rows, (q + 1) * rows)
        xs = conv_silu(pad_ref, q * full, taps, rows)
        xs_ref[out, :] = xs
        wide = xs.astype(F32)
        sent = (wide * send_ref[out, :]).astype(BF16)
        state = dot_tl(bm_ref[out, :], sent)
        state_ref[q * N : (q + 1) * N, :] = state
        state_bf_ref[q * N : (q + 1) * N, :] = state.astype(BF16)
        scaled_ref[out, :] = (wide * step_ref[out, :]).astype(BF16)


def gate_kernel(kinds, rows_w, *refs):
    x_ref = refs[0]
    pieces = refs[1 : 1 + len(kinds)]
    out_ref = refs[1 + len(kinds)]
    full = x_ref.shape[0] // 2
    z = silu(proj_pieces(x_ref, pieces, kinds, rows_w).astype(BF16).astype(F32))
    for q in range(2):
        out_ref[q * (full - HALO) : (q + 1) * (full - HALO), :] = z[q * full + HALO : (q + 1) * full]


def local_kernel(mix_ref, scaled_ref, xs_ref, skip_ref, out_ref):
    heads = mix_ref.shape[0] // 2
    rows = mix_ref.shape[1]
    size = scaled_ref.shape[1] // heads
    pack = max(1, 128 // size)
    first = my_group() * heads
    for q in range(2):
        out = slice(q * rows, (q + 1) * rows)
        for p in range(heads // pack):
            lanes = slice(p * pack * size, (p + 1) * pack * size)
            data = scaled_ref[out, lanes]
            where = lax.broadcasted_iota(jnp.int32, data.shape, 1) // size
            skip = jnp.zeros(data.shape, F32)
            total = None
            for r in range(pack):
                h = p * pack + r
                skip = jnp.where(where == r, skip_ref[first + h], skip)
                own = jnp.where(where == r, data, jnp.zeros_like(data))
                part = dot(mix_ref[q * heads + h], own)
                total = part if total is None else total + part
            out_ref[out, lanes] = total + skip * xs_ref[out, lanes].astype(F32)


def finish_kernel(kinds, cols, n_recv, slot, *refs):
    local_ref, cm_ref, reach_ref, gate_ref, scale_ref = refs[:5]
    recv = refs[5 : 5 + n_recv]
    decay = refs[5 + n_recv : 4 + 2 * n_recv]
    pieces = refs[4 + 2 * n_recv : 4 + 2 * n_recv + len(kinds)]
    out_ref, normed_ref = refs[4 + 2 * n_recv + len(kinds) :]
    rows = local_ref.shape[0] // 2
    width = local_ref.shape[1]
    c = my_group()
    mine = slice(slot * rows, (slot + 1) * rows)
    states = slice(slot * N, (slot + 1) * N)
    carry = recv[0][states, :].astype(F32)
    for r_ref, d_ref in zip(recv[1:], decay):
        carry = carry + r_ref[states, :].astype(F32) * d_ref[slot * 8 : slot * 8 + 1, :]
    reached = dot(cm_ref[mine, :], carry.astype(BF16))
    mixed = (local_ref[mine, :] + reached * reach_ref[mine, :]).astype(BF16)
    gated = mixed.astype(F32) * gate_ref[mine, :]
    mean = jnp.mean(gated * gated, axis=-1, keepdims=True)
    normed = gated * lax.rsqrt(mean + EPSILON)
    normed_ref[...] = (normed * scale_ref[:, aligned(c, width)]).astype(BF16)
    groups = {}
    for ref, (shift, flip, part) in zip(pieces, kinds):
        groups.setdefault((shift, flip), []).append((ref, part))
    for (shift, flip), members in groups.items():
        total = None
        for ref, part in members:
            if part is None:
                left = normed_ref[...]
            else:
                left = normed_ref[:, aligned(half_of(part), ref.shape[0])]
            w = ref[...] if (shift, flip) != (0, 0) else ref[aligned(c, width), :]
            piece = dot(left, w)
            total = piece if total is None else total + piece
        out_ref[:, aligned(shard_of(shift, flip), cols)] = total.astype(out_ref.dtype)


def permute(v, axis, pairs):
    return lax.ppermute(v, axis, pairs)


def gather_pieces(own, dim):
    size = lax.axis_size("dp")
    rows = own.shape[0] // (G if dim == 0 else 1)
    lanes = own.shape[1] // (G if dim == 1 else 1)
    share = lax.axis_size("grp") == 2 and rows % 256 == 0
    g = lax.axis_index("grp")
    c = my_group()

    def part(group, whole):
        at = [0, 0]
        at[dim] = group * (own.shape[dim] // G)
        depth = rows
        if share and not whole:
            depth = rows // 2
            at[0] = at[0] + g * depth
        return lax.dynamic_slice(own, at, (depth, lanes))

    pieces = [own, permute(part(1 - c, True), "dp", [(i, i ^ 1) for i in range(size)])]
    kinds = [(0, 0, None), (0, 1, None)]
    for r in range(1, size // 2):
        for flip in range(2):
            pairs = [(i, (i ^ flip) + 2 * r - size * ((i ^ flip) + 2 * r >= size)) for i in range(size)]
            a = permute(part(c ^ flip, False), "dp", pairs)
            pieces.append(a)
            if share:
                b = permute(a, "grp", [(0, 1), (1, 0)])
                pieces.append(b)
                kinds += [(2 * r, flip, 0), (2 * r, flip, 1)]
            else:
                kinds += [(2 * r, flip, None)]
    return pieces, tuple(kinds)


def call(kernel, outs, *args, scratch=(), flops=1000000, smem=()):
    specs = [
        pl.BlockSpec(memory_space=pltpu.SMEM if i in smem else pltpu.VMEM)
        for i in range(len(args))
    ]
    args = [
        v if i in smem else pltpu.with_memory_space_constraint(v, pltpu.VMEM)
        for i, v in enumerate(args)
    ]
    many = isinstance(outs, tuple)
    shapes = tuple(pltpu.VMEM(v.shape, v.dtype) for v in (outs if many else (outs,)))
    return pl.pallas_call(
        kernel,
        out_shape=shapes if many else shapes[0],
        compiler_params=pltpu.CompilerParams(vmem_limit_bytes=24 << 20),
        in_specs=specs,
        scratch_shapes=scratch,
        cost_estimate=pl.CostEstimate(flops=flops, transcendentals=0, bytes_accessed=1000000),
    )(*args)


def shards(
    mixer_source_array,
    source_projection,
    gating_projection,
    entry_mapping_projection,
    readout_mapping_projection,
    increment_projection,
    source_conv_taps,
    entry_mapping_taps,
    readout_mapping_taps,
    increment_offsets,
    channel_damping_rate,
    bypass_coefficients,
    stride_multiplier,
    added_log_damping,
    norm_scale_factor,
    final_projection,
):
    x = mixer_source_array[0]
    rows = x.shape[0]
    heads = increment_projection.shape[1] // G
    width = source_projection.shape[1] // G
    spans = lax.axis_size("sp")
    pair = [(i, i ^ 1) for i in range(lax.axis_size("dp"))]

    def forward(v, k):
        return permute(v, "sp", [(i, i + k) for i in range(spans - k)])

    src_pieces, src_kinds = gather_pieces(source_projection, 1)
    halo = forward(x[rows - HALO :], 1)
    added = added_log_damping[0].T
    added_pair = permute(added, "dp", pair)
    stride_pair = permute(stride_multiplier, "dp", pair)
    x_own = jnp.concatenate([halo, x], 0)
    x_pair = jnp.concatenate([x_own, permute(x_own, "dp", pair)], 0)

    gate_pieces, gate_kinds = gather_pieces(gating_projection, 1)
    out_pieces, out_kinds = gather_pieces(final_projection, 0)

    bm, cm, mix, step, send, reach, total = call(
        maps_kernel,
        (
            SDS((2 * rows, N), BF16),
            SDS((2 * rows, N), BF16),
            SDS((2 * heads, rows, rows), BF16),
            SDS((2 * rows, width), F32),
            SDS((2 * rows, width), F32),
            SDS((2 * rows, width), F32),
            SDS((16, width), F32),
        ),
        x_pair,
        entry_mapping_projection,
        readout_mapping_projection,
        increment_projection.T,
        entry_mapping_taps,
        readout_mapping_taps,
        increment_offsets,
        channel_damping_rate,
        stride_multiplier,
        stride_pair,
        added,
        added_pair,
        scratch=(pltpu.VMEM((2 * (rows + HALO), N), F32),),
        flops=4000000000,
        smem=(6, 7),
    )
    state_shape = (2 * N, width)
    xs, scaled, state, state_bf = call(
        functools.partial(source_kernel, src_kinds, source_projection.shape[0]),
        (
            SDS((2 * rows, width), BF16),
            SDS((2 * rows, width), BF16),
            SDS(state_shape, F32),
            SDS(state_shape, BF16),
        ),
        x_pair,
        source_conv_taps,
        step,
        send,
        bm,
        *src_pieces,
        scratch=(pltpu.VMEM((2 * (rows + HALO), width), F32),),
        flops=2000000000,
    )

    def spread_rows(v):
        factors = jnp.exp(v.reshape(2, 8, width)[:, :1])
        return jnp.broadcast_to(factors, (2, N, width)).reshape(state_shape)

    received = []
    decays = []
    window = total
    behind = None
    inclusive, inclusive_bf = state, state_bf
    k = 1
    while k < spans:
        arrived = forward(inclusive_bf, k)
        received.append(arrived)
        if behind is not None:
            decays.append(jnp.exp(behind))
        if 2 * k < spans:
            far = forward(window, k)
            inclusive = inclusive + spread_rows(window) * arrived.astype(F32)
            inclusive_bf = inclusive.astype(BF16)
            behind = far if behind is None else behind + far
            window = window + far
        k *= 2

    gate = call(
        functools.partial(gate_kernel, gate_kinds, gating_projection.shape[0]),
        SDS((2 * rows, width), F32),
        x_pair,
        *gate_pieces,
        flops=2000000000,
    )
    local = call(
        local_kernel,
        SDS((2 * rows, width), F32),
        mix,
        scaled,
        xs,
        bypass_coefficients,
        flops=3000000000,
        smem=(3,),
    )

    def finish(slot, kind):
        cols = final_projection.shape[1]
        return call(
            functools.partial(finish_kernel, out_kinds, cols, len(received), slot),
            SDS((rows, cols * lax.axis_size("dp")), kind),
            local,
            cm,
            reach,
            gate,
            norm_scale_factor[None, :],
            *received,
            *decays,
            *out_pieces,
            scratch=(pltpu.VMEM((rows, width), BF16),),
            flops=2000000000,
        )

    other = permute(finish(1, BF16), "dp", pair)
    output = (finish(0, F32) + other.astype(F32)).astype(BF16)
    return output[None]


def solution(mesh):
    return jax.shard_map(
        shards,
        mesh=mesh,
        in_specs=(
            P(("grp", "dp"), "sp", None),
            P("dp", None),
            P("dp", None),
            P(),
            P(),
            P(),
            P(),
            P(),
            P(),
            P(),
            P(),
            P(),
            P(("grp", "dp"), None),
            P(("grp", "dp"), None, None),
            P(),
            P(None, "dp"),
        ),
        out_specs=P(("grp", "dp"), "sp", None),
        check_vma=False,
    )
```

time: 155 us -> 75.8 us (0.49)
  the two profiles are of different devices: /device:TPU:0 before, /device:TPU:21 now
where the time goes in v1:
time: 75.8 us; the launch traced here: 75.5 us
  waiting for transfers between devices  27.8 us (37%)
  starting transfers between devices  26.4 us (35%)
  Pallas kernels  12.8 us (17%)
  other arithmetic  4.66 us (6%)
  local copies, waits for them, and re-layouts  3.51 us (5%)
    ppermute x23, waiting for transfers between devices, permute(): return lax.ppermute(v, axis, pairs)  27.8 us
    ppermute x23, starting transfers between devices, permute(): return lax.ppermute(v, axis, pairs)  26.4 us
    pallas_call x6, Pallas kernels, call(): pl.pallas_call(kernel, out_shape=shapes if many else shapes[0], compiler_...  12.8 us
    concatenate x1, other arithmetic, shards(): x_own = jnp.concatenate([halo, x], 0)  2.22 us
    dynamic_slice x6, local copies, waits for them, and re-layouts, part(): return lax.dynamic_slice(own, at, (depth, lanes))  1.82 us
  transfers between devices with their start and end apart: 23, of which 10 were waited for; matrix products, arithmetic and copies ran while one was open for 4% of the time, Pallas kernels for 16%

profile of v1, /device:TPU:21, one launch (start us, length us, event | category | flops | bytes accessed | tf_op | source)
XLA Modules:
  0.0 75.5 jit_solution(4219031960663375581)
XLA Ops:
  0.0 0.9 %slice_bitcast_fusion = bf16[16,2048]{1,0:T(8,128)(2,1)S(1)} fusion(bf16[1,192,2048]{2,1,0:T(8,128)(2,1)} %param.16), kind=kLoop, calls=%fused_computation.7 | loop fusion | bytes 131072 | tf_op jit(solution)/shard_map/slice | solution.py:343
  0.9 3.2 %collective-permute-start = (bf16[16,2048]{1,0:T(8,128)(2,1)S(1)}, bf16[16,2048]{1,0:T(8,128)(2,1)S(1)}, u32[]{:S(2)}, u32[]{:S(2)}) collective-permute-start(bf16[16,2048]{1,0:T(8,128)(2,1)S(1)} %slice_bitcast_fusion), channel_id=1, source_target_pairs={{0,4},{4,8},{8,12},{1,5},{5,9},{9,13},{2,6},{6,10},{10,14},{3,7},{... | collective-permute-start | bytes 196616 | tf_op jit(solution)/shard_map/ppermute | solution.py:257
  4.1 1.8 %collective-permute-done = bf16[16,2048]{1,0:T(8,128)(2,1)S(1)} collective-permute-done((bf16[16,2048]{1,0:T(8,128)(2,1)S(1)}, bf16[16,2048]{1,0:T(8,128)(2,1)S(1)}, u32[]{:S(2)}, u32[]{:S(2)}) %collective-permute-start) | collective-permute-done | bytes 65568 | tf_op jit(solution)/shard_map/ppermute | solution.py:257
  5.9 2.2 %pad_maximum_fusion.1 = bf16[208,2048]{1,0:T(8,128)(2,1)} fusion(bf16[192,2048]{1,0:T(8,128)(2,1)} %bitcast.26, bf16[16,2048]{1,0:T(8,128)(2,1)S(1)} %collective-permute-done), kind=kLoop, calls=%fused_computation.2 | loop fusion | flops 1703936 | bytes 1703936 | tf_op jit(solution)/shard_map/concatenate | solution.py:347
  8.2 1.8 %collective-permute-start.1 = (bf16[208,2048]{1,0:T(8,128)(2,1)}, bf16[208,2048]{1,0:T(8,128)(2,1)}, u32[]{:S(2)}, u32[]{:S(2)}) collective-permute-start(bf16[208,2048]{1,0:T(8,128)(2,1)} %pad_maximum_fusion.1), channel_id=1, source_target_pairs={{0,1},{1,0},{2,3},{3,2},{4,5},{5,4},{6,7},{7,6},{8,9},{9,8},{10,11... | collective-permute-start | bytes 2555912 | tf_op jit(solution)/shard_map/ppermute | solution.py:257
  10.0 0.8 %fusion.4 = (bf16[256,512]{1,0:T(8,128)(2,1)}, bf16[256,512]{1,0:T(8,128)(2,1)}) fusion(bf16[512,1024]{1,0:T(8,128)(2,1)S(1)} %copy-done.1, s32[]{:T(128)S(6)} %select_n.26, s32[]{:T(128)S(6)} %select_n.28, s32[]{:T(128)S(6)} %select_n.27), kind=kLoop, calls=%fused_computation.16 | loop fusion | bytes 1048588 | tf_op jit(solution)/shard_map/dynamic_slice | solution.py:275
  10.8 1.2 %collective-permute-start.5 = (bf16[256,512]{1,0:T(8,128)(2,1)}, bf16[256,512]{1,0:T(8,128)(2,1)S(1)}, u32[]{:S(2)}, u32[]{:S(2)}) collective-permute-start(bf16[256,512]{1,0:T(8,128)(2,1)} %get-tuple-element.32), channel_id=1, source_target_pairs={{0,2},{1,3},{2,0},{3,1},{4,6},{5,7},{6,4},{7,5},{8,10},{9,11},{10,... | collective-permute-start | bytes 786440 | tf_op jit(solution)/shard_map/ppermute | solution.py:257
  12.0 0.4 collective-permute-start.7
  12.5 0.8 %constant_dynamic-slice_fusion.4 = bf16[512,512]{1,0:T(8,128)(2,1)} fusion(bf16[512,1024]{1,0:T(8,128)(2,1)S(1)} %copy-done.1, s32[]{:T(128)S(6)} %select_n.12), kind=kLoop, calls=%fused_computation.14 | loop fusion | bytes 1048580 | tf_op jit(solution)/shard_map/dynamic_slice | solution.py:275
  13.3 0.2 collective-permute-start.4
  13.5 0.3 collective-permute-start.3
  13.9 0.0 copy-start.3
  14.0 0.3 collective-permute-start.2
  14.3 0.6 copy-done.15
  15.0 1.3 %pad_maximum_fusion.x_ref.refs_0_ = bf16[416,2048]{1,0:T(8,128)(2,1)S(1)} fusion(bf16[208,2048]{1,0:T(8,128)(2,1)} %collective-permute-done.1, bf16[192,2048]{1,0:T(8,128)(2,1)S(1)} %bitcast.27, bf16[16,2048]{1,0:T(8,128)(2,1)S(1)} %copy-done.17), kind=kLoop, calls=%fused_computation | loop fusion | flops 5111808 | bytes 3407872 | tf_op jit(solution)/shard_map/concatenate | solution.py:348
  16.2 1.3 %collective-permute-start.10 = (bf16[256,512]{1,0:T(8,128)(2,1)S(1)}, bf16[256,512]{1,0:T(8,128)(2,1)S(1)}, u32[]{:S(2)}, u32[]{:S(2)}) collective-permute-start(bf16[256,512]{1,0:T(8,128)(2,1)S(1)} %get-tuple-element.30), channel_id=1, source_target_pairs={{0,2},{1,3},{2,0},{3,1},{4,6},{5,7},{6,4},{7,5},{8,10},{9,11},{10,... | collective-permute-start | bytes 786440 | tf_op jit(solution)/shard_map/ppermute | solution.py:257
  17.5 0.6 collective-permute-start.12
  18.2 0.7 collective-permute-done.5.refs_7_
  18.9 0.2 collective-permute-start.6
  19.1 6.3 %collective-permute-done.7.refs_9_ = bf16[256,512]{1,0:T(8,128)(2,1)} collective-permute-done((bf16[256,512]{1,0:T(8,128)(2,1)}, bf16[256,512]{1,0:T(8,128)(2,1)}, u32[]{:S(2)}, u32[]{:S(2)}) %collective-permute-start.7) | collective-permute-done | bytes 262176 | tf_op jit(solution)/shard_map/ppermute | solution.py:257
  25.5 0.2 collective-permute-start.8
  25.7 5.4 %shard_map.154 = (bf16[384,128]{1,0:T(8,128)(2,1)S(1)}, bf16[384,128]{1,0:T(8,128)(2,1)S(1)}, bf16[16,192,192]{2,1,0:T(8,128)(2,1)S(1)}, f32[384,512]{1,0:T(8,12...) custom-call(bf16[416,2048]{1,0:T(8,128)(2,1)S(1)} %pad_maximum_fusion.x_ref.refs_0_, ...), custom_call_target="tpu_custom_call" | custom-call | flops 4000000000 | bytes 1000000 | tf_op jit(solution)/shard_map/pallas_call | solution.py:304
  31.2 1.2 %collective-permute-start.18 = (bf16[256,512]{1,0:T(8,128)(2,1)S(1)}, bf16[256,512]{1,0:T(8,128)(2,1)S(1)}, u32[]{:S(2)}, u32[]{:S(2)}) collective-permute-start(bf16[256,512]{1,0:T(8,128)(2,1)S(1)} %get-tuple-element.28), channel_id=1, source_target_pairs={{0,2},{1,3},{2,0},{3,1},{4,6},{5,7},{6,4},{7,5},{8,10},{9,11},{10,... | collective-permute-start | bytes 786440 | tf_op jit(solution)/shard_map/ppermute | solution.py:257
  32.4 1.6 %collective-permute-done.8.refs_10_ = bf16[256,512]{1,0:T(8,128)(2,1)S(1)} collective-permute-done((bf16[256,512]{1,0:T(8,128)(2,1)}, bf16[256,512]{1,0:T(8,128)(2,1)S(1)}, u32[]{:S(2)}, u32[]{:S(2)}) %collective-permute-start.8) | collective-permute-done | bytes 262176 | tf_op jit(solution)/shard_map/ppermute | solution.py:257
  34.0 3.4 %shard_map.155 = (bf16[384,512]{1,0:T(8,128)(2,1)S(1)}, bf16[384,512]{1,0:T(8,128)(2,1)S(1)}, f32[256,512]{1,0:T(8,128)S(1)}, bf16[256,512]{1,0:T(8,128)(2,1)S(1)}) custom-call(bf16[416,2048]{1,0:T(8,128)(2,1)S(1)} %pad_maximum_fusion.x_ref.refs_0_, f32[4,1024]{1,0:T(4,128)S(1)} %copy-done.7, f32[384,512]{1,0:T(8,128)S(1)} %get-tuple-element.17.refs_2_, ...), custom_call_target="tpu_custom_call" | custom-call | flops 2000000000 | bytes 1000000 | tf_op jit(solution)/shard_map/pallas_call | solution.py:304
  37.4 3.2 %collective-permute-start.14 = (bf16[256,512]{1,0:T(8,128)(2,1)S(1)}, bf16[256,512]{1,0:T(8,128)(2,1)S(1)}, u32[]{:S(2)}, u32[]{:S(2)}) collective-permute-start(bf16[256,512]{1,0:T(8,128)(2,1)S(1)} %get-tuple-element.24), channel_id=1, source_target_pairs={{0,4},{4,8},{8,12},{1,5},{5,9},{9,13},{2,6},{6,10},{10,14},{3,7},{... | collective-permute-start | bytes 786440 | tf_op jit(solution)/shard_map/ppermute | solution.py:257
  40.7 0.8 collective-permute-start.9
  41.4 1.2 %collective-permute-start.20 = (bf16[256,512]{1,0:T(8,128)(2,1)S(1)}, bf16[256,512]{1,0:T(8,128)(2,1)S(1)}, u32[]{:S(2)}, u32[]{:S(2)}) collective-permute-start(bf16[256,512]{1,0:T(8,128)(2,1)S(1)} %get-tuple-element.27), channel_id=1, source_target_pairs={{0,3},{1,2},{2,1},{3,0},{4,7},{5,6},{6,5},{7,4},{8,11},{9,10},{10,... | collective-permute-start | bytes 786440 | tf_op jit(solution)/shard_map/ppermute | solution.py:257
  42.6 0.2 collective-permute-start.11
  42.9 1.2 %collective-permute-start.13 = (bf16[256,512]{1,0:T(8,128)(2,1)S(1)}, bf16[256,512]{1,0:T(8,128)(2,1)S(1)}, u32[]{:S(2)}, u32[]{:S(2)}) collective-permute-start(bf16[256,512]{1,0:T(8,128)(2,1)S(1)} %collective-permute-done.12.refs_5_), channel_id=1, source_target_pairs={{0,16},{16,0},{1,17},{17,1},{2,18},{18,2},{3,19},{19,3},{4,20},{20... | collective-permute-start | bytes 786440 | tf_op jit(solution)/shard_map/ppermute | solution.py:257
  44.1 2.6 %collective-permute-done.14.refs_5_ = bf16[256,512]{1,0:T(8,128)(2,1)S(1)} collective-permute-done((bf16[256,512]{1,0:T(8,128)(2,1)S(1)}, bf16[256,512]{1,0:T(8,128)(2,1)S(1)}, u32[]{:S(2)}, u32[]{:S(2)}) %collective-permute-start.14) | collective-permute-done | bytes 262176 | tf_op jit(solution)/shard_map/ppermute | solution.py:257
  46.8 1.3 %collective-permute-start.17 = (bf16[512,512]{1,0:T(8,128)(2,1)S(1)}, bf16[512,512]{1,0:T(8,128)(2,1)S(1)}, u32[]{:S(2)}, u32[]{:S(2)}) collective-permute-start(bf16[512,512]{1,0:T(8,128)(2,1)S(1)} %constant_dynamic-slice_fusion.2), channel_id=1, source_target_pairs={{0,1},{1,0},{2,3},{3,2},{4,5},{5,4},{6,7},{7,6},{8,9},{9,8},{10,11... | collective-permute-start | bytes 1572872 | tf_op jit(solution)/shard_map/ppermute | solution.py:257
  48.1 0.1 fusion.2
  48.1 1.6 %collective-permute-done.20.refs_12_ = bf16[256,512]{1,0:T(8,128)(2,1)S(1)} collective-permute-done((bf16[256,512]{1,0:T(8,128)(2,1)S(1)}, bf16[256,512]{1,0:T(8,128)(2,1)S(1)}, u32[]{:S(2)}, u32[]{:S(2)}) %collective-permute-start.20) | collective-permute-done | bytes 262176 | tf_op jit(solution)/shard_map/ppermute | solution.py:257
  49.7 0.2 collective-permute-start.19
  50.0 0.1 collective-permute-done.11.refs_4_
  50.1 1.1 %collective-permute-start.21 = (bf16[256,512]{1,0:T(8,128)(2,1)S(1)}, bf16[256,512]{1,0:T(8,128)(2,1)S(1)}, u32[]{:S(2)}, u32[]{:S(2)}) collective-permute-start(bf16[256,512]{1,0:T(8,128)(2,1)S(1)} %collective-permute-done.20.refs_12_), channel_id=1, source_target_pairs={{0,16},{16,0},{1,17},{17,1},{2,18},{18,2},{3,19},{19,3},{4,20},{20... | collective-permute-start | bytes 786440 | tf_op jit(solution)/shard_map/ppermute | solution.py:257
  51.2 4.5 %collective-permute-done.13.refs_6_ = bf16[256,512]{1,0:T(8,128)(2,1)S(1)} collective-permute-done((bf16[256,512]{1,0:T(8,128)(2,1)S(1)}, bf16[256,512]{1,0:T(8,128)(2,1)S(1)}, u32[]{:S(2)}, u32[]{:S(2)}) %collective-permute-start.13) | collective-permute-done | bytes 262176 | tf_op jit(solution)/shard_map/ppermute | solution.py:257
  55.7 1.3 %collective-permute-start.15 = (bf16[256,512]{1,0:T(8,128)(2,1)S(1)}, bf16[256,512]{1,0:T(8,128)(2,1)S(1)}, u32[]{:S(2)}, u32[]{:S(2)}) collective-permute-start(bf16[256,512]{1,0:T(8,128)(2,1)S(1)} %fusion.2), channel_id=1, source_target_pairs={{0,8},{4,12},{1,9},{5,13},{2,10},{6,14},{3,11},{7,15},{16,24},{20,... | collective-permute-start | bytes 786440 | tf_op jit(solution)/shard_map/ppermute | solution.py:257
  57.0 1.1 %shard_map.156.refs_0_ = f32[384,512]{1,0:T(8,128)S(1)} custom-call(bf16[16,192,192]{2,1,0:T(8,128)(2,1)S(1)} %get-tuple-element.16.mix_ref, bf16[384,512]{1,0:T(8,128)(2,1)S(1)} %get-tuple-element.20.scaled_ref, bf16[384,512]{1,0:T(8,128)(2,1)S(1)} %get-tuple-element.21.xs_ref, f32[16]{0:T(128)S(1)} %copy-done.14), custom_call_target="tpu_custom_call" | custom-call | flops 3000000000 | bytes 1000000 | tf_op jit(solution)/shard_map/pallas_call | solution.py:304
  58.1 1.9 %collective-permute-start.16 = (f32[16,512]{1,0:T(8,128)S(1)}, f32[16,512]{1,0:T(8,128)S(1)}, u32[]{:S(2)}, u32[]{:S(2)}) collective-permute-start(f32[16,512]{1,0:T(8,128)S(1)} %get-tuple-element.26), channel_id=1, source_target_pairs={{0,4},{4,8},{8,12},{1,5},{5,9},{9,13},{2,6},{6,10},{10,14},{3,7},{... | collective-permute-start | bytes 98312 | tf_op jit(solution)/shard_map/ppermute | solution.py:257
  60.1 1.2 %shard_map.157.refs_3_ = f32[384,512]{1,0:T(8,128)S(1)} custom-call(bf16[416,2048]{1,0:T(8,128)(2,1)S(1)} %pad_maximum_fusion.x_ref.refs_0_, bf16[512,1024]{1,0:T(8,128)(2,1)S(1)} %copy-done.2, bf16[512,512]{1,0:T(8,128)(2,1)S(1)} %collective-permute-done.9.refs_2_, bf16[256,512]{1,0:T(8,128)(2,1)S(1)} %collective-permute-done.10.refs_3_, ...), custom_call_target="tpu_custom_call" | custom-call | flops 2000000000 | bytes 1000000 | tf_op jit(solution)/shard_map/pallas_call | solution.py:304
  61.2 7.4 %collective-permute-done.16 = f32[16,512]{1,0:T(8,128)S(1)} collective-permute-done((f32[16,512]{1,0:T(8,128)S(1)}, f32[16,512]{1,0:T(8,128)S(1)}, u32[]{:S(2)}, u32[]{:S(2)}) %collective-permute-start.16) | collective-permute-done | bytes 32800 | tf_op jit(solution)/shard_map/ppermute | solution.py:257
  68.7 0.8 %shard_map.159 = bf16[192,2048]{1,0:T(8,128)(2,1)S(1)} custom-call(f32[384,512]{1,0:T(8,128)S(1)} %shard_map.156.refs_0_, bf16[384,128]{1,0:T(8,128)(2,1)S(1)} %get-tuple-element.22.refs_1_, f32[384,512]{1,0:T(8,128)S(1)} %get-tuple-element.23.refs_2_, f32[384,512]{1,0:T(8,128)S(1)} %shard_map.157.refs_3_, f32[1,1024]{1,0:T(1,128)S(1)} %bitcast.24, ...), custom_call_target="tpu_custom_call" | custom-call | flops 2000000000 | bytes 1000000 | tf_op jit(solution)/shard_map/pallas_call | solution.py:304
  69.6 2.9 %collective-permute-start.22 = (bf16[192,2048]{1,0:T(8,128)(2,1)S(1)}, bf16[192,2048]{1,0:T(8,128)(2,1)S(1)}, u32[]{:S(2)}, u32[]{:S(2)}) collective-permute-start(bf16[192,2048]{1,0:T(8,128)(2,1)S(1)} %shard_map.159), channel_id=1, source_target_pairs={{0,1},{1,0},{2,3},{3,2},{4,5},{5,4},{6,7},{7,6},{8,9},{9,8},{10,11... | collective-permute-start | bytes 2359304 | tf_op jit(solution)/shard_map/ppermute | solution.py:257
  72.5 0.8 %shard_map.158 = f32[192,2048]{1,0:T(8,128)S(1)} custom-call(f32[384,512]{1,0:T(8,128)S(1)} %shard_map.156.refs_0_, bf16[384,128]{1,0:T(8,128)(2,1)S(1)} %get-tuple-element.22.refs_1_, f32[384,512]{1,0:T(8,128)S(1)} %get-tuple-element.23.refs_2_, f32[384,512]{1,0:T(8,128)S(1)} %shard_map.157.refs_3_, f32[1,1024]{1,0:T(1,128)S(1)} %bitcast.25, ...), custom_call_target="tpu_custom_call" | custom-call | flops 2000000000 | bytes 1000000 | tf_op jit(solution)/shard_map/pallas_call | solution.py:304
  73.3 1.1 %collective-permute-done.22 = bf16[192,2048]{1,0:T(8,128)(2,1)S(1)} collective-permute-done((bf16[192,2048]{1,0:T(8,128)(2,1)S(1)}, bf16[192,2048]{1,0:T(8,128)(2,1)S(1)}, u32[]{:S(2)}, u32[]{:S(2)}) %collective-permute-start.22) | collective-permute-done | bytes 786464 | tf_op jit(solution)/shard_map/ppermute | solution.py:257
  74.4 1.1 %fusion = bf16[1,192,2048]{2,1,0:T(8,128)(2,1)} fusion(f32[192,2048]{1,0:T(8,128)S(1)} %shard_map.158, bf16[192,2048]{1,0:T(8,128)(2,1)S(1)} %collective-permute-done.22), kind=kLoop, calls=%fused_computation.3 | loop fusion | flops 1179648 | bytes 3145728 | tf_op jit(solution)/shard_map/broadcast_in_dim | solution.py:459
  (54 shorter events, 0.3 us)
Async XLA Ops:
  0.0 10.0 %copy-start.1 = (bf16[512,1024]{1,0:T(8,128)(2,1)S(1)}, bf16[512,1024]{1,0:T(8,128)(2,1)}, u32[]{:S(2)}) copy-start(bf16[512,1024]{1,0:T(8,128)(2,1)} %refs_5_.1) | copy-start | bytes 3145732
  0.9 5.0 %collective-permute-start = (bf16[16,2048]{1,0:T(8,128)(2,1)S(1)}, bf16[16,2048]{1,0:T(8,128)(2,1)S(1)}, u32[]{:S(2)}, u32[]{:S(2)}) collective-permute-start(bf16[16,2048]{1,0:T(8,128)(2,1)S(1)} %slice_bitcast_fusion), channel_id=1, source_target_pairs={{0,4},{4,8},{8,12},{1,5},{5,9},{9,13},{2,6},{6,10},{10,14},{3,7},{... | collective-permute-start | bytes 196616 | tf_op jit(solution)/shard_map/ppermute | solution.py:257
  5.9 4.9 %copy-start.16 = (bf16[16,2048]{1,0:T(8,128)(2,1)}, bf16[16,2048]{1,0:T(8,128)(2,1)S(1)}, u32[]{:S(2)}) copy-start(bf16[16,2048]{1,0:T(8,128)(2,1)S(1)} %collective-permute-done) | copy-start | bytes 196612
  5.9 7.6 %copy-start.6 = (f32[1,768,16]{1,2,0:T(8,128)S(1)}, f32[1,768,16]{1,2,0:T(8,128)}, u32[]{:S(2)}) copy-start(f32[1,768,16]{1,2,0:T(8,128)} %param.29) | copy-start | bytes 147460
  5.9 7.9 %copy-start.2 = (bf16[512,1024]{1,0:T(8,128)(2,1)S(1)}, bf16[512,1024]{1,0:T(8,128)(2,1)}, u32[]{:S(2)}) copy-start(bf16[512,1024]{1,0:T(8,128)(2,1)} %refs_1_.3) | copy-start | bytes 3145732
  8.2 5.7 %copy-start = (bf16[1024,512]{1,0:T(8,128)(2,1)S(1)}, bf16[1024,512]{1,0:T(8,128)(2,1)}, u32[]{:S(2)}) copy-start(bf16[1024,512]{1,0:T(8,128)(2,1)} %refs_8_.3) | copy-start | bytes 3145732
  8.2 5.8 %collective-permute-start.1 = (bf16[208,2048]{1,0:T(8,128)(2,1)}, bf16[208,2048]{1,0:T(8,128)(2,1)}, u32[]{:S(2)}, u32[]{:S(2)}) collective-permute-start(bf16[208,2048]{1,0:T(8,128)(2,1)} %pad_maximum_fusion.1), channel_id=1, source_target_pairs={{0,1},{1,0},{2,3},{3,2},{4,5},{5,4},{6,7},{7,6},{8,9},{9,8},{10,11... | collective-permute-start | bytes 2555912 | tf_op jit(solution)/shard_map/ppermute | solution.py:257
  10.8 3.2 %copy-start.11 = (f32[1,768]{1,0:T(1,128)S(1)}, f32[1,768]{1,0:T(1,128)}, u32[]{:S(2)}) copy-start(f32[1,768]{1,0:T(1,128)} %stride0_ref.1) | copy-start | bytes 9220
  10.8 8.1 %collective-permute-start.5 = (bf16[256,512]{1,0:T(8,128)(2,1)}, bf16[256,512]{1,0:T(8,128)(2,1)S(1)}, u32[]{:S(2)}, u32[]{:S(2)}) collective-permute-start(bf16[256,512]{1,0:T(8,128)(2,1)} %get-tuple-element.32), channel_id=1, source_target_pairs={{0,2},{1,3},{2,0},{3,1},{4,6},{5,7},{6,4},{7,5},{8,10},{9,11},{10,... | collective-permute-start | bytes 786440 | tf_op jit(solution)/shard_map/ppermute | solution.py:257
  12.0 13.4 %collective-permute-start.7 = (bf16[256,512]{1,0:T(8,128)(2,1)}, bf16[256,512]{1,0:T(8,128)(2,1)}, u32[]{:S(2)}, u32[]{:S(2)}) collective-permute-start(bf16[256,512]{1,0:T(8,128)(2,1)} %get-tuple-element.31), channel_id=1, source_target_pairs={{0,3},{1,2},{2,1},{3,0},{4,7},{5,6},{6,5},{7,4},{8,11},{9,10},{10,... | collective-permute-start | bytes 786440 | tf_op jit(solution)/shard_map/ppermute | solution.py:257
  13.3 20.7 %collective-permute-start.4 = (bf16[512,512]{1,0:T(8,128)(2,1)}, bf16[512,512]{1,0:T(8,128)(2,1)}, u32[]{:S(2)}, u32[]{:S(2)}) collective-permute-start(bf16[512,512]{1,0:T(8,128)(2,1)} %constant_dynamic-slice_fusion.4), channel_id=1, source_target_pairs={{0,1},{1,0},{2,3},{3,2},{4,5},{5,4},{6,7},{7,6},{8,9},{9,8},{10,11... | collective-permute-start | bytes 1572872 | tf_op jit(solution)/shard_map/ppermute | solution.py:257
  13.5 4.0 %collective-permute-start.3 = (f32[16,768]{1,0:T(8,128)S(1)}, f32[16,768]{1,0:T(8,128)S(1)}, u32[]{:S(2)}, u32[]{:S(2)}) collective-permute-start(f32[16,768]{1,0:T(8,128)S(1)} %bitcast.22), channel_id=1, source_target_pairs={{0,1},{1,0},{2,3},{3,2},{4,5},{5,4},{6,7},{7,6},{8,9},{9,8},{10,11... | collective-permute-start | bytes 147464 | tf_op jit(solution)/shard_map/ppermute | solution.py:257
  13.8 1.1 %copy-start.15 = (bf16[1,192,2048]{2,1,0:T(8,128)(2,1)S(1)}, bf16[1,192,2048]{2,1,0:T(8,128)(2,1)}, u32[]{:S(2)}) copy-start(bf16[1,192,2048]{2,1,0:T(8,128)(2,1)} %param.16) | copy-start | bytes 2359300
  13.8 1.1 %copy-start.17 = (bf16[16,2048]{1,0:T(8,128)(2,1)S(1)}, bf16[16,2048]{1,0:T(8,128)(2,1)}, u32[]{:S(2)}) copy-start(bf16[16,2048]{1,0:T(8,128)(2,1)} %copy-done.16) | copy-start | bytes 196612
  13.9 11.8 %copy-start.3 = (bf16[2048,256]{1,0:T(8,128)(2,1)S(1)}, bf16[2048,256]{1,0:T(8,128)(2,1)}, u32[]{:S(2)}) copy-start(bf16[2048,256]{1,0:T(8,128)(2,1)} %wb_ref.1) | copy-start | bytes 3145732
  13.9 11.7 %copy-start.4 = (bf16[2048,256]{1,0:T(8,128)(2,1)S(1)}, bf16[2048,256]{1,0:T(8,128)(2,1)}, u32[]{:S(2)}) copy-start(bf16[2048,256]{1,0:T(8,128)(2,1)} %wc_ref.1) | copy-start | bytes 3145732
  14.0 11.7 %copy-start.5 = (bf16[2048,16]{0,1:T(8,128)(2,1)S(1)}, bf16[2048,16]{0,1:T(8,128)(2,1)}, u32[]{:S(2)}) copy-start(bf16[2048,16]{0,1:T(8,128)(2,1)} %param.21) | copy-start | bytes 196612
  14.0 11.7 %copy-start.8 = (f32[4,256]{1,0:T(4,128)S(1)}, f32[4,256]{1,0:T(4,128)}, u32[]{:S(2)}) copy-start(f32[4,256]{1,0:T(4,128)} %taps_b_ref.1) | copy-start | bytes 12292
  14.0 11.7 %copy-start.9 = (f32[4,256]{1,0:T(4,128)S(1)}, f32[4,256]{1,0:T(4,128)}, u32[]{:S(2)}) copy-start(f32[4,256]{1,0:T(4,128)} %taps_c_ref.1) | copy-start | bytes 12292
  14.0 11.7 %copy-start.12 = (f32[16]{0:T(128)S(1)}, f32[16]{0:T(128)}, u32[]{:S(2)}) copy-start(f32[16]{0:T(128)} %offset_ref.1) | copy-start | bytes 196
  14.0 11.7 %copy-start.13 = (f32[16]{0:T(128)S(1)}, f32[16]{0:T(128)}, u32[]{:S(2)}) copy-start(f32[16]{0:T(128)} %rate_ref.1) | copy-start | bytes 196
  14.0 2.2 %collective-permute-start.2 = (f32[1,768]{1,0:T(1,128)S(1)}, f32[1,768]{1,0:T(1,128)S(1)}, u32[]{:S(2)}, u32[]{:S(2)}) collective-permute-start(f32[1,768]{1,0:T(1,128)S(1)} %copy-done.11), channel_id=1, source_target_pairs={{0,1},{1,0},{2,3},{3,2},{4,5},{5,4},{6,7},{7,6},{8,9},{9,8},{10,11... | collective-permute-start | bytes 9224 | tf_op jit(solution)/shard_map/ppermute | solution.py:257
  16.2 25.2 %collective-permute-start.10 = (bf16[256,512]{1,0:T(8,128)(2,1)S(1)}, bf16[256,512]{1,0:T(8,128)(2,1)S(1)}, u32[]{:S(2)}, u32[]{:S(2)}) collective-permute-start(bf16[256,512]{1,0:T(8,128)(2,1)S(1)} %get-tuple-element.30), channel_id=1, source_target_pairs={{0,2},{1,3},{2,0},{3,1},{4,6},{5,7},{6,4},{7,5},{8,10},{9,11},{10,... | collective-permute-start | bytes 786440 | tf_op jit(solution)/shard_map/ppermute | solution.py:257
  17.5 25.1 %collective-permute-start.12 = (bf16[256,512]{1,0:T(8,128)(2,1)S(1)}, bf16[256,512]{1,0:T(8,128)(2,1)S(1)}, u32[]{:S(2)}, u32[]{:S(2)}) collective-permute-start(bf16[256,512]{1,0:T(8,128)(2,1)S(1)} %get-tuple-element.29), channel_id=1, source_target_pairs={{0,3},{1,2},{2,1},{3,0},{4,7},{5,6},{6,5},{7,4},{8,11},{9,10},{10,... | collective-permute-start | bytes 786440 | tf_op jit(solution)/shard_map/ppermute | solution.py:257
  18.9 12.3 %collective-permute-start.6 = (bf16[256,512]{1,0:T(8,128)(2,1)S(1)}, bf16[256,512]{1,0:T(8,128)(2,1)S(1)}, u32[]{:S(2)}, u32[]{:S(2)}) collective-permute-start(bf16[256,512]{1,0:T(8,128)(2,1)S(1)} %collective-permute-done.5.refs_7_), channel_id=1, source_target_pairs={{0,16},{16,0},{1,17},{17,1},{2,18},{18,2},{3,19},{19,3},{4,20},{20... | collective-permute-start | bytes 786440 | tf_op jit(solution)/shard_map/ppermute | solution.py:257
  25.5 8.5 %collective-permute-start.8 = (bf16[256,512]{1,0:T(8,128)(2,1)}, bf16[256,512]{1,0:T(8,128)(2,1)S(1)}, u32[]{:S(2)}, u32[]{:S(2)}) collective-permute-start(bf16[256,512]{1,0:T(8,128)(2,1)} %collective-permute-done.7.refs_9_), channel_id=1, source_target_pairs={{0,16},{16,0},{1,17},{17,1},{2,18},{18,2},{3,19},{19,3},{4,20},{20... | collective-permute-start | bytes 786440 | tf_op jit(solution)/shard_map/ppermute | solution.py:257
  25.7 8.3 %copy-start.7 = (f32[4,1024]{1,0:T(4,128)S(1)}, f32[4,1024]{1,0:T(4,128)}, u32[]{:S(2)}) copy-start(f32[4,1024]{1,0:T(4,128)} %refs_1_.2) | copy-start | bytes 49156
  31.2 11.7 %collective-permute-start.18 = (bf16[256,512]{1,0:T(8,128)(2,1)S(1)}, bf16[256,512]{1,0:T(8,128)(2,1)S(1)}, u32[]{:S(2)}, u32[]{:S(2)}) collective-permute-start(bf16[256,512]{1,0:T(8,128)(2,1)S(1)} %get-tuple-element.28), channel_id=1, source_target_pairs={{0,2},{1,3},{2,0},{3,1},{4,6},{5,7},{6,4},{7,5},{8,10},{9,11},{10,... | collective-permute-start | bytes 786440 | tf_op jit(solution)/shard_map/ppermute | solution.py:257
  37.4 19.6 %copy-start.14 = (f32[16]{0:T(128)S(1)}, f32[16]{0:T(128)}, u32[]{:S(2)}) copy-start(f32[16]{0:T(128)} %skip_ref.1) | copy-start | bytes 196
  37.4 9.4 %collective-permute-start.14 = (bf16[256,512]{1,0:T(8,128)(2,1)S(1)}, bf16[256,512]{1,0:T(8,128)(2,1)S(1)}, u32[]{:S(2)}, u32[]{:S(2)}) collective-permute-start(bf16[256,512]{1,0:T(8,128)(2,1)S(1)} %get-tuple-element.24), channel_id=1, source_target_pairs={{0,4},{4,8},{8,12},{1,5},{5,9},{9,13},{2,6},{6,10},{10,14},{3,7},{... | collective-permute-start | bytes 786440 | tf_op jit(solution)/shard_map/ppermute | solution.py:257
  40.7 17.4 %collective-permute-start.9 = (bf16[512,512]{1,0:T(8,128)(2,1)S(1)}, bf16[512,512]{1,0:T(8,128)(2,1)S(1)}, u32[]{:S(2)}, u32[]{:S(2)}) collective-permute-start(bf16[512,512]{1,0:T(8,128)(2,1)S(1)} %constant_dynamic-slice_fusion.3), channel_id=1, source_target_pairs={{0,1},{1,0},{2,3},{3,2},{4,5},{5,4},{6,7},{7,6},{8,9},{9,8},{10,11... | collective-permute-start | bytes 1572872 | tf_op jit(solution)/shard_map/ppermute | solution.py:257
  41.4 8.3 %collective-permute-start.20 = (bf16[256,512]{1,0:T(8,128)(2,1)S(1)}, bf16[256,512]{1,0:T(8,128)(2,1)S(1)}, u32[]{:S(2)}, u32[]{:S(2)}) collective-permute-start(bf16[256,512]{1,0:T(8,128)(2,1)S(1)} %get-tuple-element.27), channel_id=1, source_target_pairs={{0,3},{1,2},{2,1},{3,0},{4,7},{5,6},{6,5},{7,4},{8,11},{9,10},{10,... | collective-permute-start | bytes 786440 | tf_op jit(solution)/shard_map/ppermute | solution.py:257
  42.6 7.4 %collective-permute-start.11 = (bf16[256,512]{1,0:T(8,128)(2,1)S(1)}, bf16[256,512]{1,0:T(8,128)(2,1)S(1)}, u32[]{:S(2)}, u32[]{:S(2)}) collective-permute-start(bf16[256,512]{1,0:T(8,128)(2,1)S(1)} %collective-permute-done.10.refs_3_), channel_id=1, source_target_pairs={{0,16},{16,0},{1,17},{17,1},{2,18},{18,2},{3,19},{19,3},{4,20},{20... | collective-permute-start | bytes 786440 | tf_op jit(solution)/shard_map/ppermute | solution.py:257
  42.9 12.8 %collective-permute-start.13 = (bf16[256,512]{1,0:T(8,128)(2,1)S(1)}, bf16[256,512]{1,0:T(8,128)(2,1)S(1)}, u32[]{:S(2)}, u32[]{:S(2)}) collective-permute-start(bf16[256,512]{1,0:T(8,128)(2,1)S(1)} %collective-permute-done.12.refs_5_), channel_id=1, source_target_pairs={{0,16},{16,0},{1,17},{17,1},{2,18},{18,2},{3,19},{19,3},{4,20},{20... | collective-permute-start | bytes 786440 | tf_op jit(solution)/shard_map/ppermute | solution.py:257
  46.8 21.9 %collective-permute-start.17 = (bf16[512,512]{1,0:T(8,128)(2,1)S(1)}, bf16[512,512]{1,0:T(8,128)(2,1)S(1)}, u32[]{:S(2)}, u32[]{:S(2)}) collective-permute-start(bf16[512,512]{1,0:T(8,128)(2,1)S(1)} %constant_dynamic-slice_fusion.2), channel_id=1, source_target_pairs={{0,1},{1,0},{2,3},{3,2},{4,5},{5,4},{6,7},{7,6},{8,9},{9,8},{10,11... | collective-permute-start | bytes 1572872 | tf_op jit(solution)/shard_map/ppermute | solution.py:257
  49.7 18.9 %collective-permute-start.19 = (bf16[256,512]{1,0:T(8,128)(2,1)S(1)}, bf16[256,512]{1,0:T(8,128)(2,1)S(1)}, u32[]{:S(2)}, u32[]{:S(2)}) collective-permute-start(bf16[256,512]{1,0:T(8,128)(2,1)S(1)} %collective-permute-done.18.refs_10_), channel_id=1, source_target_pairs={{0,16},{16,0},{1,17},{17,1},{2,18},{18,2},{3,19},{19,3},{4,20},{20... | collective-permute-start | bytes 786440 | tf_op jit(solution)/shard_map/ppermute | solution.py:257
  50.1 18.6 %collective-permute-start.21 = (bf16[256,512]{1,0:T(8,128)(2,1)S(1)}, bf16[256,512]{1,0:T(8,128)(2,1)S(1)}, u32[]{:S(2)}, u32[]{:S(2)}) collective-permute-start(bf16[256,512]{1,0:T(8,128)(2,1)S(1)} %collective-permute-done.20.refs_12_), channel_id=1, source_target_pairs={{0,16},{16,0},{1,17},{17,1},{2,18},{18,2},{3,19},{19,3},{4,20},{20... | collective-permute-start | bytes 786440 | tf_op jit(solution)/shard_map/ppermute | solution.py:257
  55.7 13.0 %collective-permute-start.15 = (bf16[256,512]{1,0:T(8,128)(2,1)S(1)}, bf16[256,512]{1,0:T(8,128)(2,1)S(1)}, u32[]{:S(2)}, u32[]{:S(2)}) collective-permute-start(bf16[256,512]{1,0:T(8,128)(2,1)S(1)} %fusion.2), channel_id=1, source_target_pairs={{0,8},{4,12},{1,9},{5,13},{2,10},{6,14},{3,11},{7,15},{16,24},{20,... | collective-permute-start | bytes 786440 | tf_op jit(solution)/shard_map/ppermute | solution.py:257
  58.1 10.6 %copy-start.10 = (f32[1024]{0:T(1024)S(1)}, f32[1024]{0:T(1024)}, u32[]{:S(2)}) copy-start(f32[1024]{0:T(1024)} %param.30) | copy-start | bytes 12292
  58.1 10.5 %collective-permute-start.16 = (f32[16,512]{1,0:T(8,128)S(1)}, f32[16,512]{1,0:T(8,128)S(1)}, u32[]{:S(2)}, u32[]{:S(2)}) collective-permute-start(f32[16,512]{1,0:T(8,128)S(1)} %get-tuple-element.26), channel_id=1, source_target_pairs={{0,4},{4,8},{8,12},{1,5},{5,9},{9,13},{2,6},{6,10},{10,14},{3,7},{... | collective-permute-start | bytes 98312 | tf_op jit(solution)/shard_map/ppermute | solution.py:257
  69.6 4.8 %collective-permute-start.22 = (bf16[192,2048]{1,0:T(8,128)(2,1)S(1)}, bf16[192,2048]{1,0:T(8,128)(2,1)S(1)}, u32[]{:S(2)}, u32[]{:S(2)}) collective-permute-start(bf16[192,2048]{1,0:T(8,128)(2,1)S(1)} %shard_map.159), channel_id=1, source_target_pairs={{0,1},{1,0},{2,3},{3,2},{4,5},{5,4},{6,7},{7,6},{8,9},{9,8},{10,11... | collective-permute-start | bytes 2359304 | tf_op jit(solution)/shard_map/ppermute | solution.py:257
